TPU v7x, 32 devices: a whole 2x2x4 slice. The times are simulated.
32 devices in a mesh: sp: 8 (over z, y), dp: 4 (over x, core).
Axes of the slice: x: 2, y: 2, z: 4, core: 2. Of those that a mesh axis runs over, the one named last changes fastest.
Arguments:
- tokens: bfloat16 [4, 512, 1024], P('dp', 'sp'), may hold values from -6 to 6
- w_query: bfloat16 [1024, 512], P(None, ('sp', 'dp')), may hold values from -0.1875 to 0.1875
- w_forward: bfloat16 [1024, 512], P(None, ('sp', 'dp')), may hold values from -0.1875 to 0.1875
- w_backward: bfloat16 [1024, 512], P(None, ('sp', 'dp')), may hold values from -0.1875 to 0.1875
- w_input: bfloat16 [1024, 512], P(None, ('sp', 'dp')), may hold values from -0.1875 to 0.1875
- w_gate: bfloat16 [1024, 512], P(None, ('sp', 'dp')), may hold values from -0.1875 to 0.1875
- w_out: bfloat16 [512, 1024], P(None, ('sp', 'dp')), may hold values from -0.25 to 0.25
- memory_forward: float32 [512], replicated, may hold values from 0.3 to 4
- memory_backward: float32 [512], replicated, may hold values from 0.3 to 4
- norm_gain: float32 [128], replicated, may hold values from 0.1 to 1.9
Outputs:
- mixed: bfloat16 [4, 512, 1024], P('dp', 'sp')
All inputs are finite; a program needn't handle non-finite values.
Results may differ from a plain program's by a relative error of at most 0.015.
Values may be sent and summed in bfloat16 or wider, within the bound.
A program may use at most 64 MiB of HBM per device.

v0:
```python
import jax
import jax.numpy as jnp
from jax import lax
from jax.sharding import PartitionSpec as P

HEADS = 4
HEAD_DIM = 128
BLOCK = 64


norm_eps = 1e-06
highest = lax.Precision.HIGHEST


def as_sent(array):
    return jax.tree.map(lambda a: a.astype(jnp.bfloat16) if a.dtype == jnp.float32 else a, array)


def gathered_then(share, axis, dim, apply):
    everything = lax.all_gather(share, axis, axis=dim, tiled=True)
    return apply(everything, jnp.int32(0))


def log_forget(projected, memory, seq_len):
    slack_value = memory / seq_len
    return jnp.logaddexp(
        jnp.log1p(-slack_value),
        jnp.log(slack_value) + jax.nn.log_sigmoid(projected.astype(jnp.float32)),
    )


def sweep(queries, log_decay, values):
    seq_len, key_width = queries.shape
    blocks = seq_len // BLOCK
    input_keys = -jnp.expm1(log_decay)
    lower_mask = jnp.tril(jnp.ones((BLOCK, BLOCK), dtype=bool))[:, :, None]

    def advance(carry_state, inputs):
        query_part, decay_part, key_part, value_part = inputs
        running = jnp.cumsum(decay_part, axis=0)
        from_state = jnp.dot(query_part * jnp.exp(running), carry_state, precision=highest)
        gaps = running[:, None, :] - running[None, :, :]
        decay_table = jnp.where(lower_mask, jnp.exp(jnp.where(lower_mask, gaps, 0.0)), 0.0)
        scores = jnp.sum(query_part[:, None, :] * key_part[None, :, :] * decay_table, axis=2)
        inside = jnp.dot(scores, value_part, precision=highest)
        final_sum = running[-1]
        weighted = key_part * jnp.exp(final_sum[None, :] - running)
        carry_state = jnp.exp(final_sum)[:, None] * carry_state + jnp.dot(
            weighted.T, value_part, precision=highest
        )
        return (carry_state, from_state + inside)

    def blocked(array):
        return array.reshape(blocks, BLOCK, array.shape[1])

    zero_state = jnp.zeros((key_width, values.shape[1]), jnp.float32)
    _, readings = lax.scan(
        advance,
        zero_state,
        (blocked(queries), blocked(log_decay), blocked(input_keys), blocked(values)),
    )
    return readings.reshape(seq_len, values.shape[1])


def both_ways(queries, log_ahead, log_behind, values):
    forward_read = sweep(queries, log_ahead, values)
    behind = sweep(jnp.flip(queries, 0), jnp.flip(log_behind, 0), jnp.flip(values, 0))
    return forward_read + jnp.flip(behind, 0)


def body(
    tokens,
    w_query,
    w_forward,
    w_backward,
    w_input,
    w_gate,
    w_out,
    memory_forward,
    memory_backward,
    norm_gain,
):
    seq_count, tok_count, model_width = tokens.shape
    row_count = seq_count * tok_count
    flat_tokens = tokens.reshape(row_count, model_width)
    group_count = lax.axis_size("sp")
    per_head_groups = group_count // HEADS
    block_width = HEAD_DIM // per_head_groups
    head_index = lax.axis_index("sp") // per_head_groups
    full_query, full_forward, full_backward, full_input, full_gate = (
        lax.all_gather(w_query, ("sp", "dp"), axis=1, tiled=True),
        lax.all_gather(w_forward, ("sp", "dp"), axis=1, tiled=True),
        lax.all_gather(w_backward, ("sp", "dp"), axis=1, tiled=True),
        lax.all_gather(w_input, ("sp", "dp"), axis=1, tiled=True),
        lax.all_gather(w_gate, ("sp", "dp"), axis=1, tiled=True),
    )

    def project(weight):
        return jnp.dot(flat_tokens, weight, preferred_element_type=jnp.float32).astype(jnp.bfloat16)

    def by_head(projected):
        shaped = projected.reshape(row_count, HEADS, 1, HEAD_DIM)
        spread_out = jnp.broadcast_to(shaped, (row_count, HEADS, per_head_groups, HEAD_DIM))
        return spread_out.reshape(row_count, group_count, HEAD_DIM)

    def by_group(projected):
        return projected.reshape(row_count, group_count, block_width)

    query_heads, ahead_heads, behind_heads, value_heads = (
        lax.all_to_all(
            as_sent(by_head(project(full_query))), "sp", split_axis=1, concat_axis=0, tiled=True
        ),
        lax.all_to_all(
            as_sent(by_head(project(full_forward))), "sp", split_axis=1, concat_axis=0, tiled=True
        ),
        lax.all_to_all(
            as_sent(by_head(project(full_backward))), "sp", split_axis=1, concat_axis=0, tiled=True
        ),
        lax.all_to_all(
            as_sent(by_group(project(full_input))), "sp", split_axis=1, concat_axis=0, tiled=True
        ),
    )
    gate_rows = project(full_gate)
    seq_len = query_heads.shape[0]
    memory_ahead = lax.dynamic_slice_in_dim(memory_forward, head_index * HEAD_DIM, HEAD_DIM)
    memory_behind = lax.dynamic_slice_in_dim(memory_backward, head_index * HEAD_DIM, HEAD_DIM)
    queries = jax.nn.silu(query_heads[:, 0].astype(jnp.float32))
    log_ahead = log_forget(ahead_heads[:, 0], memory_ahead, seq_len)
    log_behind = log_forget(behind_heads[:, 0], memory_behind, seq_len)
    values = value_heads[:, 0].astype(jnp.float32)
    readout = both_ways(queries, log_ahead, log_behind, values).astype(jnp.bfloat16)
    returned = lax.all_to_all(
        readout.reshape(seq_len, 1, block_width), "sp", split_axis=0, concat_axis=1, tiled=True
    )
    readout_rows = returned.reshape(row_count, HEADS, HEAD_DIM).astype(jnp.float32)
    normed = (
        readout_rows
        * lax.rsqrt(jnp.mean(readout_rows * readout_rows, axis=-1, keepdims=True) + norm_eps)
        * norm_gain
    )
    normed = normed.reshape(row_count, HEADS * HEAD_DIM)
    gated_rows = (normed * jax.nn.silu(gate_rows.astype(jnp.float32))).astype(jnp.bfloat16)

    def output_block(weight_piece, first_index):
        return jnp.dot(gated_rows, weight_piece, preferred_element_type=jnp.float32).astype(
            jnp.bfloat16
        )

    mixed_rows = gathered_then(w_out, ("sp", "dp"), 1, output_block)
    return mixed_rows.reshape(seq_count, tok_count, model_width)


def solution(mesh):
    return jax.shard_map(
        body,
        mesh=mesh,
        in_specs=(
            P("dp", "sp", None),
            P(None, ("sp", "dp")),
            P(None, ("sp", "dp")),
            P(None, ("sp", "dp")),
            P(None, ("sp", "dp")),
            P(None, ("sp", "dp")),
            P(None, ("sp", "dp")),
            P(),
            P(),
            P(),
        ),
        out_specs=P("dp", "sp", None),
        check_vma=False,
    )
```

profile of v0, /device:TPU:0, one launch (start us, length us, event | category | flops | bytes accessed | tf_op | source)
XLA Modules:
  0.0 353.6 jit_solution(13744162278260831660)
XLA Ops:
  12.1 54.4 %all-gather.13.cloned.1.call-done = bf16[1024,512]{0,1:T(8,128)(2,1)} async-done(((bf16[1024,16]{0,1:T(8,128)(2,1)}), bf16[1024,512]{0,1:T(8,128)(2,1)}) %all-gather.13.cloned.1.call-update) | async-done | bytes 1048592 | tf_op jit(solution)/shard_map/all_gather | solution.py:93
  66.5 1.7 fusion.54
  68.2 53.7 %all-gather.9.cloned.1.call-done = bf16[1024,512]{0,1:T(8,128)(2,1)} async-done(((bf16[1024,16]{0,1:T(8,128)(2,1)}), bf16[1024,512]{0,1:T(8,128)(2,1)}) %all-gather.9.cloned.1.call-update) | async-done | bytes 1048592 | tf_op jit(solution)/shard_map/all_gather | solution.py:94
  121.9 1.7 convolution_convert_fusion.4
  124.5 4.5 %all-to-all-start.1 = ((bf16[8,2,2048]{2,1,0:T(2,128)(2,1)}), bf16[8,2,2048]{2,1,0:T(2,128)(2,1)S(1)}, u32[]{:S(2)}, u32[]{:S(2)}) async-start(bf16[8,2,2048]{2,1,0:T(2,128)(2,1)} %reshape.264), calls=%async_computation.1 | async-start | bytes 131072 | tf_op jit(solution)/shard_map/all_to_all | solution.py:119
  129.0 48.3 %all-gather.11.cloned.1.call-done = bf16[1024,512]{0,1:T(8,128)(2,1)} async-done(((bf16[1024,16]{0,1:T(8,128)(2,1)}), bf16[1024,512]{0,1:T(8,128)(2,1)}) %all-gather.11.cloned.1.call-update) | async-done | bytes 1048592 | tf_op jit(solution)/shard_map/all_gather | solution.py:91
  177.2 1.7 fusion.53
  178.9 53.5 %all-gather.7.cloned.1.call-done = bf16[1024,512]{0,1:T(8,128)(2,1)} async-done(((bf16[1024,16]{0,1:T(8,128)(2,1)}), bf16[1024,512]{0,1:T(8,128)(2,1)}) %all-gather.7.cloned.1.call-update) | async-done | bytes 1048592 | tf_op jit(solution)/shard_map/all_gather | solution.py:92
  232.5 1.7 fusion.52
  234.8 4.5 %all-to-all-start.3 = ((bf16[64,8,128]{2,0,1:T(8,128)(2,1)}), bf16[64,8,128]{2,0,1:T(8,128)(2,1)S(1)}, u32[]{:S(2)}, u32[]{:S(2)}) async-start(bf16[64,8,128]{2,0,1:T(8,128)(2,1)} %bitcast.17), calls=%async_computation.3 | async-start | bytes 262144 | tf_op jit(solution)/shard_map/all_to_all | solution.py:116
  239.7 7.0 %all-to-all-done.3 = bf16[64,8,128]{2,0,1:T(8,128)(2,1)S(1)} async-done(((bf16[64,8,128]{2,0,1:T(8,128)(2,1)}), bf16[64,8,128]{2,0,1:T(8,128)(2,1)S(1)}, u32[]{:S(2)}, u32[]{:S(2)}) %all-to-all-start.3) | async-done | bytes 131104 | tf_op jit(solution)/shard_map/all_to_all | solution.py:116
  247.4 3.4 all-to-all-start.2
  251.3 6.7 %all-to-all-done.2 = bf16[64,8,128]{2,0,1:T(8,128)(2,1)S(1)} async-done(((bf16[64,8,128]{2,0,1:T(8,128)(2,1)}), bf16[64,8,128]{2,0,1:T(8,128)(2,1)S(1)}, u32[]{:S(2)}, u32[]{:S(2)}) %all-to-all-start.2) | async-done | bytes 131104 | tf_op jit(solution)/shard_map/all_to_all | solution.py:110
  258.7 3.4 all-to-all-start
  262.3 17.5 %while.29 = (s32[]{:T(128)}, f32[128,64]{0,1:T(8,128)S(1)}, f32[8,64,64]{2,1,0:T(8,128)S(1)}, f32[8,64,128]{2,1,0:T(8,128)S(1)}, f32[8,64,128]{2,1,0:T(8,128)S(1...) while((s32[]{:T(128)}, f32[128,64]{0,1:T(8,128)S(1)}, ...), condition=%wide.region_7.8_spmd.clone.clone, body=%wide.region_4.7_spmd.clone.clone.sunk | while | flops 19451908 | bytes 799868 | solution.py:57
  264.7 1.4 multiply_reduce_fusion.6
  271.2 1.4 multiply_reduce_fusion.6
  280.4 17.5 %while.28 = (s32[]{:T(128)}, f32[128,64]{0,1:T(8,128)S(1)}, f32[8,64,64]{2,1,0:T(8,128)S(1)}, f32[8,64,128]{2,1,0:T(8,128)S(1)}, f32[8,64,128]{2,1,0:T(8,128)S(1...) while((s32[]{:T(128)}, f32[128,64]{0,1:T(8,128)S(1)}, ...), condition=%wide.region_3.4_spmd.clone.clone, body=%wide.region_0.3_spmd.clone.clone.sunk | while | flops 19451908 | bytes 799868 | solution.py:57
  280.5 1.4 multiply_reduce_fusion.5
  293.6 1.4 multiply_reduce_fusion.5
  300.6 5.9 %all-to-all-start.4 = ((bf16[8,2,2048]{2,1,0:T(2,128)(2,1)}), bf16[8,2,2048]{2,1,0:T(2,128)(2,1)S(1)}, u32[]{:S(2)}, u32[]{:S(2)}) async-start(bf16[8,2,2048]{2,1,0:T(2,128)(2,1)} %reshape.266), calls=%async_computation.4 | async-start | bytes 131072 | tf_op jit(solution)/shard_map/all_to_all | solution.py:132
  306.5 6.9 %all-to-all-done.4 = bf16[8,2,2048]{2,1,0:T(2,128)(2,1)S(1)} async-done(((bf16[8,2,2048]{2,1,0:T(2,128)(2,1)}), bf16[8,2,2048]{2,1,0:T(2,128)(2,1)S(1)}, u32[]{:S(2)}, u32[]{:S(2)}) %all-to-all-start.4) | async-done | bytes 65568 | tf_op jit(solution)/shard_map/all_to_all | solution.py:132
  314.3 29.2 %all-gather.17.cloned.1.call-done = bf16[512,1024]{0,1:T(8,128)(2,1)} async-done(((bf16[512,32]{0,1:T(8,128)(2,1)}), bf16[512,1024]{0,1:T(8,128)(2,1)}) %all-gather.17.cloned.1.call-update) | async-done | bytes 1048592 | tf_op jit(solution)/shard_map/all_gather | solution.py:20
  343.7 3.0 fusion.50
  (221 shorter events, 41.8 us)
Async XLA Ops:
  6.5 60.0 %copy-start = (bf16[1,64,1024]{2,1,0:T(8,128)(2,1)S(1)}, bf16[1,64,1024]{2,1,0:T(8,128)(2,1)}, u32[]{:S(2)}) copy-start(bf16[1,64,1024]{2,1,0:T(8,128)(2,1)} %param.14) | copy-start | bytes 393220
  6.5 59.9 %all-gather.13.cloned.1.call-start = ((), (), s32[]{:S(2)}) async-start(), calls=%async_computation.8 | async-start | bytes 1081344 | tf_op jit(solution)/shard_map/all_gather | solution.py:93
  7.3 114.6 %all-gather.9.cloned.1.call-start = ((), (), s32[]{:S(2)}) async-start(), calls=%async_computation.6 | async-start | bytes 1081344 | tf_op jit(solution)/shard_map/all_gather | solution.py:94
  8.0 169.2 %all-gather.11.cloned.1.call-start = ((), (), s32[]{:S(2)}) async-start(), calls=%async_computation.7 | async-start | bytes 1081344 | tf_op jit(solution)/shard_map/all_gather | solution.py:91
  8.7 223.7 %all-gather.7.cloned.1.call-start = ((), (), s32[]{:S(2)}) async-start(), calls=%async_computation.5 | async-start | bytes 1081344 | tf_op jit(solution)/shard_map/all_gather | solution.py:92
  9.3 305.0 %all-gather.15.cloned.1.call-start = ((), (), s32[]{:S(2)}) async-start(), calls=%async_computation.9 | async-start | bytes 1081344 | tf_op jit(solution)/shard_map/all_gather | solution.py:95
  9.9 333.6 %all-gather.17.cloned.1.call-start = ((), (), s32[]{:S(2)}) async-start(), calls=%async_computation.10 | async-start | bytes 1081344 | tf_op jit(solution)/shard_map/all_gather | solution.py:20
  124.5 109.7 %all-to-all-start.1 = ((bf16[8,2,2048]{2,1,0:T(2,128)(2,1)}), bf16[8,2,2048]{2,1,0:T(2,128)(2,1)S(1)}, u32[]{:S(2)}, u32[]{:S(2)}) async-start(bf16[8,2,2048]{2,1,0:T(2,128)(2,1)} %reshape.264), calls=%async_computation.1 | async-start | bytes 131072 | tf_op jit(solution)/shard_map/all_to_all | solution.py:119
  234.8 11.9 %all-to-all-start.3 = ((bf16[64,8,128]{2,0,1:T(8,128)(2,1)}), bf16[64,8,128]{2,0,1:T(8,128)(2,1)S(1)}, u32[]{:S(2)}, u32[]{:S(2)}) async-start(bf16[64,8,128]{2,0,1:T(8,128)(2,1)} %bitcast.17), calls=%async_computation.3 | async-start | bytes 262144 | tf_op jit(solution)/shard_map/all_to_all | solution.py:116
  247.4 10.7 %all-to-all-start.2 = ((bf16[64,8,128]{2,0,1:T(8,128)(2,1)}), bf16[64,8,128]{2,0,1:T(8,128)(2,1)S(1)}, u32[]{:S(2)}, u32[]{:S(2)}) async-start(bf16[64,8,128]{2,0,1:T(8,128)(2,1)} %bitcast.10), calls=%async_computation.2 | async-start | bytes 262144 | tf_op jit(solution)/shard_map/all_to_all | solution.py:110
  258.7 21.2 %all-to-all-start = ((bf16[64,8,128]{2,0,1:T(8,128)(2,1)}), bf16[64,8,128]{2,0,1:T(8,128)(2,1)S(1)}, u32[]{:S(2)}, u32[]{:S(2)}) async-start(bf16[64,8,128]{2,0,1:T(8,128)(2,1)} %bitcast.1), calls=%async_computation | async-start | bytes 262144 | tf_op jit(solution)/shard_map/all_to_all | solution.py:113
  297.8 8.7 %copy-start.1 = (f32[128]{0:T(128)S(1)}, f32[128]{0:T(128)}, u32[]{:S(2)}) copy-start(f32[128]{0:T(128)} %param.23) | copy-start | bytes 1540
  300.6 12.8 %all-to-all-start.4 = ((bf16[8,2,2048]{2,1,0:T(2,128)(2,1)}), bf16[8,2,2048]{2,1,0:T(2,128)(2,1)S(1)}, u32[]{:S(2)}, u32[]{:S(2)}) async-start(bf16[8,2,2048]{2,1,0:T(2,128)(2,1)} %reshape.266), calls=%async_computation.4 | async-start | bytes 131072 | tf_op jit(solution)/shard_map/all_to_all | solution.py:132
Sparse Core Ops, SparseCore 0:
  10.2 56.2 all-gather.12
  69.3 52.4 all-gather.8
  124.7 52.4 all-gather.10
  180.0 52.4 all-gather.6
  235.2 53.0 all-gather.14
  291.0 52.5 all-gather.16
where the time goes:
time: 354 us
  waiting for transfers between devices  263 us (74%)
  other arithmetic  26.9 us (8%)
  starting transfers between devices  21.9 us (6%)
  matrix products  19.3 us (5%)
  between operations  13.8 us (4%)
  local copies, waits for them, and re-layouts  6.91 us (2%)
    all_gather x1, waiting for transfers between devices, body(): lax.all_gather(w_backward, ('sp', 'dp'), axis=1, tiled=True)  54.4 us
    all_gather x1, waiting for transfers between devices, body(): lax.all_gather(w_input, ('sp', 'dp'), axis=1, tiled=True)  53.7 us
    all_gather x1, waiting for transfers between devices, body(): lax.all_gather(w_forward, ('sp', 'dp'), axis=1, tiled=True)  53.5 us
    all_gather x1, waiting for transfers between devices, body(): lax.all_gather(w_query, ('sp', 'dp'), axis=1, tiled=True)  48.3 us
    all_gather x1, waiting for transfers between devices, gathered_then(): everything = lax.all_gather(share, axis, axis=dim, tiled=True)  29.2 us
    reduce_sum x16, other arithmetic, advance(): jnp.sum(query_part[:, None, :] * key_part[None, :, :] * decay_table, axis=2)  21.8 us
  transfers between devices with their start and end apart: 11, of which 8 were waited for; matrix products, arithmetic and copies ran while one was open for 14% of the time, Pallas kernels for 0%

commit v1 on v0

--- a/solution.py
+++ b/solution.py
@@ -1,6 +1,10 @@
+import functools
+
 import jax
 import jax.numpy as jnp
 from jax import lax
+from jax.experimental import pallas as pl
+from jax.experimental.pallas import tpu as pltpu
 from jax.sharding import PartitionSpec as P
 
 HEADS = 4
@@ -150,9 +154,379 @@
     return mixed_rows.reshape(seq_count, tok_count, model_width)
 
 
+def dot_nt(left, right):
+    return lax.dot_general(
+        left, right, (((1,), (1,)), ((), ())), preferred_element_type=jnp.float32
+    )
+
+
+def layer_kernel(
+    members,
+    columns,
+    tokens,
+    w_query,
+    w_forward,
+    w_backward,
+    w_input,
+    w_gate,
+    w_out,
+    memory_forward,
+    memory_backward,
+    norm_gain,
+    mixed,
+    token_all,
+    weight_all,
+    out_all,
+    raw,
+    mixed_heads,
+    gated_own,
+    sum_mask,
+    token_send,
+    token_recv,
+    weight_send,
+    weight_recv,
+    relay_send,
+    relay_recv,
+    out_send,
+    out_recv,
+    plane_send,
+    plane_recv,
+    back_send,
+    back_recv,
+    raw_send,
+    raw_recv,
+    gated_send,
+    gated_recv,
+    local_sem,
+):
+    bf16, f32 = jnp.bfloat16, jnp.float32
+    block = tokens.shape[0]
+    own_rows = HEADS * block
+    sp, dp = lax.axis_index("sp"), lax.axis_index("dp")
+    head, member = sp // members, lax.rem(sp, members)
+    column, core = dp // 2, lax.rem(dp, 2)
+    seq_len = own_rows * members
+
+    def turned(index, step, size):
+        return lax.rem(index + step, size)
+
+    def device(h, r, x, c):
+        return {"sp": h * members + r, "dp": x * 2 + c}
+
+    plane = [(a, b) for a in range(members) for b in range(columns) if (a, b) != (0, 0)]
+    plane.sort(key=lambda ab: -((ab[0] != 0) + (ab[1] != 0)))
+
+    def remote(src, dst, send, recv, where):
+        return pltpu.make_async_remote_copy(
+            src_ref=src,
+            dst_ref=dst,
+            send_sem=send,
+            recv_sem=recv,
+            device_id=where,
+            device_id_type=pl.DeviceIdType.MESH,
+        )
+
+    across = [device(turned(head, k, HEADS), member, column, core) for k in range(1, HEADS)]
+    beside = [
+        device(head, turned(member, a, members), turned(column, b, columns), core)
+        for a, b in plane
+    ]
+    partner = device(head, member, column, 1 - core)
+
+    barrier = pltpu.get_barrier_semaphore()
+    for where in across + beside + [partner]:
+        pl.semaphore_signal(barrier, inc=1, device_id=where, device_id_type=pl.DeviceIdType.MESH)
+    pl.semaphore_wait(barrier, len(across) + len(beside) + 1)
+
+    weights = (w_query, w_forward, w_backward, w_input, w_gate)
+    token_copies = []
+    for k in range(1, HEADS):
+        copy = remote(
+            tokens,
+            token_all.at[head],
+            token_send.at[k - 1],
+            token_recv.at[k - 1],
+            across[k - 1],
+        )
+        copy.start()
+        token_copies.append(copy)
+    weight_copies = []
+    for i, where in enumerate(beside + [partner]):
+        for j, weight in enumerate(weights):
+            copy = remote(
+                weight,
+                weight_all.at[j, member, dp],
+                weight_send.at[i],
+                weight_recv.at[i],
+                where,
+            )
+            copy.start()
+    out_copies = []
+    for k in range(1, HEADS):
+        copy = remote(
+            w_out,
+            out_all.at[head, member, dp],
+            out_send.at[k - 1],
+            out_recv.at[k - 1],
+            across[k - 1],
+        )
+        copy.start()
+        out_copies.append(copy)
+    local = [
+        pltpu.make_async_copy(tokens, token_all.at[head], local_sem.at[0]),
+        pltpu.make_async_copy(w_out, out_all.at[head, member, dp], local_sem.at[1]),
+    ]
+    for j, weight in enumerate(weights):
+        local.append(
+            pltpu.make_async_copy(weight, weight_all.at[j, member, dp], local_sem.at[2 + j])
+        )
+    for copy in local:
+        copy.start()
+
+    def places(shape, dim, slot):
+        row = lax.broadcasted_iota(jnp.int32, shape, dim)
+        return (row // block) * (members * block) + lax.rem(row, block) + turned(
+            member, slot, members
+        ) * block
+
+    for a in range(members):
+        for b in range(members):
+            shape = (own_rows, own_rows)
+            earlier = places(shape, 1, b) <= places(shape, 0, a)
+            sum_mask[a * own_rows : (a + 1) * own_rows, b * own_rows : (b + 1) * own_rows] = (
+                jnp.where(earlier, 1.0, 0.0).astype(bf16)
+            )
+
+    for copy in local:
+        copy.wait()
+
+    def weight_block(r, x, c):
+        return weight_all.at[:, r, x * 2 + c]
+
+    relays = []
+    for i, (a, b) in enumerate(plane):
+        r = turned(member, members - a, members)
+        x = turned(column, columns - b, columns)
+        landed = weight_block(r, x, core)
+        remote(landed, landed, weight_send.at[i], weight_recv.at[i], partner).wait_recv()
+        copy = remote(landed, landed, relay_send.at[i], relay_recv.at[i], partner)
+        copy.start()
+        relays.append(copy)
+    last = len(plane)
+    landed = weight_block(member, column, 1 - core)
+    remote(landed, landed, weight_send.at[last], weight_recv.at[last], partner).wait_recv()
+    for copy in relays:
+        copy.wait_recv()
+    for copy in token_copies:
+        copy.wait_recv()
+
+    depth = tokens.shape[1]
+    rows = token_all[...].reshape(own_rows, depth)
+
+    def project(first, count):
+        weight = weight_all[first : first + count].reshape(count * HEAD_DIM, depth)
+        return dot_nt(rows, weight).astype(bf16)
+
+    sent = project(1, 3)
+    for j in range(3):
+        raw[0, j] = sent[:, j * HEAD_DIM : (j + 1) * HEAD_DIM]
+    raw_copies = []
+    for a in range(1, members):
+        copy = remote(
+            raw.at[0],
+            raw.at[members - a],
+            raw_send.at[a - 1],
+            raw_recv.at[a - 1],
+            device(head, turned(member, a, members), column, core),
+        )
+        copy.start()
+        raw_copies.append(copy)
+    for copy in out_copies:
+        copy.wait_recv()
+    plane_copies = []
+    mine = out_all.at[:, member, dp]
+    for i, where in enumerate(beside + [partner]):
+        copy = remote(mine, mine, plane_send.at[i], plane_recv.at[i], where)
+        copy.start()
+        plane_copies.append(copy)
+
+    gate = project(4, 1).astype(f32)
+    query = project(0, 1).astype(f32)
+    queries = query * jax.nn.sigmoid(query)
+    gate = gate * jax.nn.sigmoid(gate)
+
+    for copy in raw_copies:
+        copy.wait_recv()
+
+    channels = pl.ds(pl.multiple_of(head * HEAD_DIM, HEAD_DIM), HEAD_DIM)
+
+    def keys_of(j, memory):
+        slack_value = memory[:, channels] / seq_len
+        projected = raw[:, j].reshape(seq_len, HEAD_DIM).astype(f32)
+        key = slack_value * jax.nn.sigmoid(-projected)
+        return key, jnp.log1p(-key)
+
+    key_ahead, log_ahead = keys_of(0, memory_forward)
+    key_behind, log_behind = keys_of(1, memory_backward)
+    values = raw[:, 2].reshape(seq_len, HEAD_DIM)
+    logs = jnp.concatenate([log_ahead, log_behind], axis=1)
+    coarse = logs.astype(bf16)
+    fine = (logs - coarse.astype(f32)).astype(bf16)
+    sums = jnp.dot(
+        sum_mask[...], jnp.concatenate([coarse, fine], axis=1), preferred_element_type=f32
+    )
+    sums = sums[:, : 2 * HEAD_DIM] + sums[:, 2 * HEAD_DIM :]
+    ahead = sums[:, :HEAD_DIM]
+    behind = sums[:, HEAD_DIM:] - log_behind
+    query_ahead = (queries * jnp.exp(ahead[:own_rows])).astype(bf16)
+    query_behind = (queries * jnp.exp(-behind[:own_rows])).astype(bf16)
+    key_ahead = (key_ahead * jnp.exp(-ahead)).astype(bf16)
+    key_behind = (key_behind * jnp.exp(behind)).astype(bf16)
+
+    readout = jnp.zeros((own_rows, HEAD_DIM), f32)
+    for b in range(members):
+        part = slice(b * own_rows, (b + 1) * own_rows)
+        shape = (own_rows, own_rows)
+        there, here = places(shape, 1, b), places(shape, 0, 0)
+        scores = jnp.where(there <= here, dot_nt(query_ahead, key_ahead[part]), 0.0) + jnp.where(
+            there >= here, dot_nt(query_behind, key_behind[part]), 0.0
+        )
+        readout = readout + jnp.dot(
+            scores.astype(bf16), values[part], preferred_element_type=f32
+        )
+    readout = readout.astype(bf16).astype(f32)
+    square = jnp.mean(readout * readout, axis=-1, keepdims=True)
+    gated = (readout * lax.rsqrt(square + norm_eps) * norm_gain[...] * gate).astype(bf16)
+    gated_own[...] = gated.reshape(HEADS, block, HEAD_DIM)
+
+    gated_copies = []
+    for k in range(1, HEADS):
+        copy = remote(
+            gated_own.at[turned(head, k, HEADS)],
+            mixed_heads.at[head],
+            gated_send.at[k - 1],
+            gated_recv.at[k - 1],
+            across[k - 1],
+        )
+        copy.start()
+        gated_copies.append(copy)
+    own = pltpu.make_async_copy(gated_own.at[head], mixed_heads.at[head], local_sem.at[0])
+    own.start()
+
+    back_copies = []
+    for i, (a, b) in enumerate(plane):
+        r = turned(member, members - a, members)
+        x = turned(column, columns - b, columns)
+        plane_copies[i].wait_recv()
+        landed = out_all.at[:, r, x * 2 + core]
+        copy = remote(landed, landed, back_send.at[i], back_recv.at[i], partner)
+        copy.start()
+        back_copies.append(copy)
+    plane_copies[last].wait_recv()
+    for copy in back_copies:
+        copy.wait_recv()
+    own.wait()
+    for copy in gated_copies:
+        copy.wait_recv()
+
+    total = jnp.zeros((block, depth), f32)
+    weight = out_all[...].reshape(depth, HEADS * HEAD_DIM)
+    joined = jnp.concatenate([mixed_heads[h] for h in range(HEADS)], axis=1)
+    mixed[...] = dot_nt(joined, weight).astype(bf16)
+
+    for copy in token_copies + relays + out_copies + plane_copies + back_copies:
+        copy.wait_send()
+    for copy in raw_copies + gated_copies:
+        copy.wait_send()
+    mine = weight_block(member, column, core)
+    for i in range(last + 1):
+        remote(mine, mine, weight_send.at[i], weight_recv.at[i], partner).wait_send()
+
+
+def whole_layer(
+    members,
+    columns,
+    tokens,
+    w_query,
+    w_forward,
+    w_backward,
+    w_input,
+    w_gate,
+    w_out,
+    memory_forward,
+    memory_backward,
+    norm_gain,
+):
+    _, block, depth = tokens.shape
+    width = w_query.shape[1]
+    out_width = w_out.shape[1]
+    own_rows = HEADS * block
+    seq_len = own_rows * members
+    others = HEADS - 1
+    beside = members * columns
+    bf16 = jnp.bfloat16
+    dma = pltpu.SemaphoreType.DMA
+    vmem = pl.BlockSpec(memory_space=pltpu.VMEM)
+    flat = pl.pallas_call(
+        functools.partial(layer_kernel, members, columns),
+        out_shape=jax.ShapeDtypeStruct((block, depth), bf16),
+        in_specs=[vmem] * 10,
+        out_specs=vmem,
+        scratch_shapes=[
+            pltpu.VMEM((HEADS, block, depth), bf16),
+            pltpu.VMEM((5, members, 2 * columns, width, depth), bf16),
+            pltpu.VMEM((HEADS, members, 2 * columns, out_width, HEADS * HEAD_DIM), bf16),
+            pltpu.VMEM((members, 3, own_rows, HEAD_DIM), bf16),
+            pltpu.VMEM((HEADS, block, HEAD_DIM), bf16),
+            pltpu.VMEM((HEADS, block, HEAD_DIM), bf16),
+            pltpu.VMEM((seq_len, seq_len), bf16),
+            dma((others,)),
+            dma((others,)),
+            dma((beside,)),
+            dma((beside,)),
+            dma((beside,)),
+            dma((beside,)),
+            dma((others,)),
+            dma((others,)),
+            dma((beside,)),
+            dma((beside,)),
+            dma((beside,)),
+            dma((beside,)),
+            dma((members,)),
+            dma((members,)),
+            dma((others,)),
+            dma((others,)),
+            dma((7,)),
+        ],
+        compiler_params=pltpu.CompilerParams(
+            collective_id=0, has_side_effects=True, vmem_limit_bytes=48 * 1024 * 1024
+        ),
+    )(
+        tokens.reshape(block, depth),
+        w_query.T,
+        w_forward.T,
+        w_backward.T,
+        w_input.T,
+        w_gate.T,
+        w_out.T,
+        memory_forward.reshape(1, -1),
+        memory_backward.reshape(1, -1),
+        norm_gain.reshape(1, -1),
+    )
+    return flat.reshape(1, block, depth)
+
+
+def layer(mesh, tokens, w_query, *rest):
+    members = mesh.shape["sp"] // HEADS
+    columns = mesh.shape["dp"] // 2
+    if tokens.shape[0] == 1 and w_query.shape[1] % 16 == 0:
+        return whole_layer(members, columns, tokens, w_query, *rest)
+    return body(tokens, w_query, *rest)
+
+
 def solution(mesh):
     return jax.shard_map(
-        body,
+        functools.partial(layer, mesh),
         mesh=mesh,
         in_specs=(
             P("dp", "sp", None),

time: 354 us -> 42.6 us (0.12)
  waiting for transfers between devices: 263 us -> 0 us
  Pallas kernels: 0 us -> 35.2 us
  other arithmetic: 26.9 us -> 0 us
  starting transfers between devices: 21.9 us -> 0 us
  matrix products: 19.3 us -> 0 us
  between operations: 13.8 us -> 0.02 us
    all_gather x6 -> x0, waiting for transfers between devices: 239 us -> none  [the longest x1 54.4 us: body(): lax.all_gather(w_backward, ('sp', 'dp'), axis=1, tiled=True)]
    pallas_call x0 -> x1, Pallas kernels: none -> 35.2 us  [whole_layer(): pl.pallas_call(functools.partial(layer_kernel, members, columns), out_sha...]
    reduce_sum x18 -> x0, other arithmetic: 21.9 us -> none  [the longest x16 21.8 us: advance(): jnp.sum(query_part[:, None, :] * key_part[None, :, :] * decay_table, axis=2)]
    all_to_all x5 -> x0, starting transfers between devices: 21.7 us -> none  [the longest x1 5.93 us: body(): lax.all_to_all(readout.reshape(seq_len, 1, block_width), 'sp', split_axis...]
    all_to_all x5 -> x0, waiting for transfers between devices: 20.6 us -> none  [the longest x1 7.04 us: body(): lax.all_to_all(as_sent(by_head(project(full_backward))), 'sp', split_axis...]
    dot_general x53 -> x0, matrix products: 19.3 us -> none  [the longest x4 6.66 us: project(): jnp.dot(flat_tokens, weight, preferred_element_type=jnp.float32)]
    unnamed x9 -> x21, local copies, waits for them, and re-layouts: 2 us -> 6.8 us
    unnamed x6 -> x0, waiting for transfers between devices: 3.67 us -> none
  transfers between devices with their start and end apart: 11 -> 0, of which waited for: 8 -> 0; matrix products, arithmetic and copies ran while one was open for 14% -> 0% of each run, Pallas kernels for 0% -> 0%
where the time goes in v1:
time: 42.6 us; the launch traced here: 42.1 us
  Pallas kernels  35.2 us (83%)
  local copies, waits for them, and re-layouts  6.8 us (16%)
    pallas_call x1, Pallas kernels, whole_layer(): pl.pallas_call(functools.partial(layer_kernel, members, columns), out_sha...  35.2 us
    unnamed x21, local copies, waits for them, and re-layouts  6.8 us

profile of v1, /device:TPU:0, one launch (start us, length us, event | category | flops | bytes accessed | tf_op | source)
XLA Modules:
  0.0 42.1 jit_solution(9628488285824559210)
XLA Ops:
  0.0 0.0 copy-start.8
  0.0 0.0 copy-start.7
  0.0 0.0 copy-start.9
  0.0 0.7 %copy-done.8 = f32[512]{0:T(512)S(1)} copy-done((f32[512]{0:T(512)S(1)}, f32[512]{0:T(512)}, u32[]{:S(2)}) %copy-start.8) | copy-done | bytes 2072
  0.7 0.0 copy-done.7
  0.7 0.0 copy-done.9
  0.7 0.0 copy-start
  0.7 0.9 %copy-done = bf16[1,64,1024]{2,1,0:T(8,128)(2,1)S(1)} copy-done((bf16[1,64,1024]{2,1,0:T(8,128)(2,1)S(1)}, bf16[1,64,1024]{2,1,0:T(8,128)(2,1)}, u32[]{:S(2)}) %copy-start) | copy-done | bytes 131096
  1.6 0.0 copy-start.1
  1.6 0.8 %copy-done.1 = bf16[1024,16]{0,1:T(8,128)(2,1)S(1)} copy-done((bf16[1024,16]{0,1:T(8,128)(2,1)S(1)}, bf16[1024,16]{0,1:T(8,128)(2,1)}, u32[]{:S(2)}) %copy-start.1) | copy-done | bytes 32792
  2.4 0.0 copy-start.2
  2.4 0.8 %copy-done.2 = bf16[1024,16]{0,1:T(8,128)(2,1)S(1)} copy-done((bf16[1024,16]{0,1:T(8,128)(2,1)S(1)}, bf16[1024,16]{0,1:T(8,128)(2,1)}, u32[]{:S(2)}) %copy-start.2) | copy-done | bytes 32792
  3.1 0.0 copy-start.3
  3.1 0.8 %copy-done.3 = bf16[1024,16]{0,1:T(8,128)(2,1)S(1)} copy-done((bf16[1024,16]{0,1:T(8,128)(2,1)S(1)}, bf16[1024,16]{0,1:T(8,128)(2,1)}, u32[]{:S(2)}) %copy-start.3) | copy-done | bytes 32792
  3.9 0.0 copy-start.4
  3.9 0.8 %copy-done.4 = bf16[1024,16]{0,1:T(8,128)(2,1)S(1)} copy-done((bf16[1024,16]{0,1:T(8,128)(2,1)S(1)}, bf16[1024,16]{0,1:T(8,128)(2,1)}, u32[]{:S(2)}) %copy-start.4) | copy-done | bytes 32792
  4.6 0.0 copy-start.5
  4.6 0.8 %copy-done.5 = bf16[1024,16]{0,1:T(8,128)(2,1)S(1)} copy-done((bf16[1024,16]{0,1:T(8,128)(2,1)S(1)}, bf16[1024,16]{0,1:T(8,128)(2,1)}, u32[]{:S(2)}) %copy-start.5) | copy-done | bytes 32792
  5.4 0.0 copy-start.6
  5.4 0.8 %copy-done.6 = bf16[512,32]{0,1:T(8,128)(2,1)S(1)} copy-done((bf16[512,32]{0,1:T(8,128)(2,1)S(1)}, bf16[512,32]{0,1:T(8,128)(2,1)}, u32[]{:S(2)}) %copy-start.6) | copy-done | bytes 32792
  6.2 35.2 %shard_map.100 = bf16[64,1024]{1,0:T(8,128)(2,1)S(1)} custom-call(bf16[64,1024]{1,0:T(8,128)(2,1)S(1)} %bitcast.12, bf16[16,1024]{1,0:T(8,128)(2,1)S(1)} %bitcast.13, bf16[16,1024]{1,0:T(8,128)(2,1)S(1)} %bitcast.14, bf16[16,1024]{1,0:T(8,128)(2,1)S(1)} %bitcast.15, bf16[16,1024]{1,0:T(8,128)(2,1)S(1)} %bitcast.16, bf16[16,1024]{1,0:T(8,128)(2,1)S(1)} %bitcast.17, ...), custom_call_target="tpu_custom_call" | custom-call | tf_op jit(solution)/shard_map/pallas_call | solution.py:470
  41.4 0.7 %copy.12 = bf16[1,64,1024]{2,1,0:T(8,128)(2,1)} copy(bf16[1,64,1024]{2,1,0:T(8,128)(2,1)S(1)} %bitcast.11) | data formatting | bytes 262144
Async XLA Ops:
  0.0 0.7 %copy-start.8 = (f32[512]{0:T(512)S(1)}, f32[512]{0:T(512)}, u32[]{:S(2)}) copy-start(f32[512]{0:T(512)} %param.18) | copy-start | bytes 6148
  0.0 0.7 %copy-start.7 = (f32[512]{0:T(512)S(1)}, f32[512]{0:T(512)}, u32[]{:S(2)}) copy-start(f32[512]{0:T(512)} %param.17) | copy-start | bytes 6148
  0.0 0.7 %copy-start.9 = (f32[128]{0:T(128)S(1)}, f32[128]{0:T(128)}, u32[]{:S(2)}) copy-start(f32[128]{0:T(128)} %param.19) | copy-start | bytes 1540
  0.7 0.9 %copy-start = (bf16[1,64,1024]{2,1,0:T(8,128)(2,1)S(1)}, bf16[1,64,1024]{2,1,0:T(8,128)(2,1)}, u32[]{:S(2)}) copy-start(bf16[1,64,1024]{2,1,0:T(8,128)(2,1)} %param.10) | copy-start | bytes 393220
  1.6 0.8 %copy-start.1 = (bf16[1024,16]{0,1:T(8,128)(2,1)S(1)}, bf16[1024,16]{0,1:T(8,128)(2,1)}, u32[]{:S(2)}) copy-start(bf16[1024,16]{0,1:T(8,128)(2,1)} %param.11) | copy-start | bytes 98308
  2.4 0.8 %copy-start.2 = (bf16[1024,16]{0,1:T(8,128)(2,1)S(1)}, bf16[1024,16]{0,1:T(8,128)(2,1)}, u32[]{:S(2)}) copy-start(bf16[1024,16]{0,1:T(8,128)(2,1)} %param.12) | copy-start | bytes 98308
  3.1 0.8 %copy-start.3 = (bf16[1024,16]{0,1:T(8,128)(2,1)S(1)}, bf16[1024,16]{0,1:T(8,128)(2,1)}, u32[]{:S(2)}) copy-start(bf16[1024,16]{0,1:T(8,128)(2,1)} %param.13) | copy-start | bytes 98308
  3.9 0.8 %copy-start.4 = (bf16[1024,16]{0,1:T(8,128)(2,1)S(1)}, bf16[1024,16]{0,1:T(8,128)(2,1)}, u32[]{:S(2)}) copy-start(bf16[1024,16]{0,1:T(8,128)(2,1)} %param.14) | copy-start | bytes 98308
  4.6 0.8 %copy-start.5 = (bf16[1024,16]{0,1:T(8,128)(2,1)S(1)}, bf16[1024,16]{0,1:T(8,128)(2,1)}, u32[]{:S(2)}) copy-start(bf16[1024,16]{0,1:T(8,128)(2,1)} %param.15) | copy-start | bytes 98308
  5.4 0.8 %copy-start.6 = (bf16[512,32]{0,1:T(8,128)(2,1)S(1)}, bf16[512,32]{0,1:T(8,128)(2,1)}, u32[]{:S(2)}) copy-start(bf16[512,32]{0,1:T(8,128)(2,1)} %param.16) | copy-start | bytes 98308

commit v2 on v1

--- a/solution.py
+++ b/solution.py
@@ -154,6 +154,9 @@
     return mixed_rows.reshape(seq_count, tok_count, model_width)
 
 
+GROUPS = ((0, 1, 2), (3,))
+
+
 def dot_nt(left, right):
     return lax.dot_general(
         left, right, (((1,), (1,)), ((), ())), preferred_element_type=jnp.float32
@@ -174,6 +177,9 @@
     memory_backward,
     norm_gain,
     mixed,
+    small,
+    gain,
+    query_gate,
     token_all,
     weight_all,
     out_all,
@@ -200,12 +206,14 @@
     local_sem,
 ):
     bf16, f32 = jnp.bfloat16, jnp.float32
-    block = tokens.shape[0]
+    block, depth = tokens.shape
+    half = block // 2
     own_rows = HEADS * block
     sp, dp = lax.axis_index("sp"), lax.axis_index("dp")
     head, member = sp // members, lax.rem(sp, members)
     column, core = dp // 2, lax.rem(dp, 2)
     seq_len = own_rows * members
+    heads = (head, head + 1 - 2 * lax.rem(head, 2), lax.rem(head + 2, HEADS), HEADS - 1 - head)
 
     def turned(index, step, size):
         return lax.rem(index + step, size)
@@ -215,6 +223,7 @@
 
     plane = [(a, b) for a in range(members) for b in range(columns) if (a, b) != (0, 0)]
     plane.sort(key=lambda ab: -((ab[0] != 0) + (ab[1] != 0)))
+    last = len(plane)
 
     def remote(src, dst, send, recv, where):
         return pltpu.make_async_remote_copy(
@@ -226,62 +235,74 @@
             device_id_type=pl.DeviceIdType.MESH,
         )
 
-    across = [device(turned(head, k, HEADS), member, column, core) for k in range(1, HEADS)]
+    across = [device(heads[k], member, column, core) for k in range(HEADS)]
     beside = [
         device(head, turned(member, a, members), turned(column, b, columns), core)
         for a, b in plane
     ]
     partner = device(head, member, column, 1 - core)
 
+    weights = (w_query, w_forward, w_backward, w_input, w_gate)
+    local = []
+    for j, weight in enumerate(weights):
+        local.append(pltpu.make_async_copy(weight, weight_all.at[j, member, dp], local_sem.at[j]))
+    local.append(pltpu.make_async_copy(tokens, token_all.at[0], local_sem.at[5]))
+    local.append(
+        pltpu.make_async_copy(w_out, out_all.at[head, member, dp], local_sem.at[6])
+    )
+    local.append(pltpu.make_async_copy(memory_forward, small.at[0:1], local_sem.at[7]))
+    local.append(pltpu.make_async_copy(memory_backward, small.at[1:2], local_sem.at[8]))
+    local.append(pltpu.make_async_copy(norm_gain, gain, local_sem.at[9]))
+    for copy in [local[5]] + local[:5] + local[6:]:
+        copy.start()
+
     barrier = pltpu.get_barrier_semaphore()
-    for where in across + beside + [partner]:
+    greeted = across[1:] + beside + [partner]
+    for where in greeted:
         pl.semaphore_signal(barrier, inc=1, device_id=where, device_id_type=pl.DeviceIdType.MESH)
-    pl.semaphore_wait(barrier, len(across) + len(beside) + 1)
-
-    weights = (w_query, w_forward, w_backward, w_input, w_gate)
+    pl.semaphore_wait(barrier, len(greeted))
+
     token_copies = []
-    for k in range(1, HEADS):
-        copy = remote(
-            tokens,
-            token_all.at[head],
-            token_send.at[k - 1],
-            token_recv.at[k - 1],
-            across[k - 1],
-        )
-        copy.start()
-        token_copies.append(copy)
+    local[5].wait()
+
+    def rows_of(k, piece):
+        return token_all.at[k, piece * half : (piece + 1) * half]
+
+    def send_tokens(source, slot, where):
+        for piece in range(2):
+            at = 2 * (slot - 1) + piece
+            copy = remote(
+                rows_of(source, piece),
+                rows_of(slot, piece),
+                token_send.at[at],
+                token_recv.at[at],
+                where,
+            )
+            token_copies.append(copy)
+
+    send_tokens(0, 1, across[1])
+    send_tokens(0, 2, across[2])
+    for copy in token_copies:
+        copy.start()
+
+    def weight_block(r, x, c):
+        return weight_all.at[:, r, x * 2 + c]
+
+    for copy in local[:5]:
+        copy.wait()
+    mine = weight_block(member, column, core)
     weight_copies = []
     for i, where in enumerate(beside + [partner]):
-        for j, weight in enumerate(weights):
-            copy = remote(
-                weight,
-                weight_all.at[j, member, dp],
-                weight_send.at[i],
-                weight_recv.at[i],
-                where,
-            )
-            copy.start()
+        copy = remote(mine, mine, weight_send.at[i], weight_recv.at[i], where)
+        copy.start()
+        weight_copies.append(copy)
+    local[6].wait()
+    out_mine = out_all.at[head, member, dp]
     out_copies = []
-    for k in range(1, HEADS):
-        copy = remote(
-            w_out,
-            out_all.at[head, member, dp],
-            out_send.at[k - 1],
-            out_recv.at[k - 1],
-            across[k - 1],
-        )
+    for k in (1, 2):
+        copy = remote(out_mine, out_mine, out_send.at[k - 1], out_recv.at[k - 1], across[k])
         copy.start()
         out_copies.append(copy)
-    local = [
-        pltpu.make_async_copy(tokens, token_all.at[head], local_sem.at[0]),
-        pltpu.make_async_copy(w_out, out_all.at[head, member, dp], local_sem.at[1]),
-    ]
-    for j, weight in enumerate(weights):
-        local.append(
-            pltpu.make_async_copy(weight, weight_all.at[j, member, dp], local_sem.at[2 + j])
-        )
-    for copy in local:
-        copy.start()
 
     def places(shape, dim, slot):
         row = lax.broadcasted_iota(jnp.int32, shape, dim)
@@ -297,52 +318,65 @@
                 jnp.where(earlier, 1.0, 0.0).astype(bf16)
             )
 
-    for copy in local:
-        copy.wait()
-
-    def weight_block(r, x, c):
-        return weight_all.at[:, r, x * 2 + c]
+    send_tokens(2, 3, across[1])
+    for piece in range(2):
+        token_copies[2 + piece].wait_recv()
+        token_copies[4 + piece].start()
 
     relays = []
     for i, (a, b) in enumerate(plane):
         r = turned(member, members - a, members)
         x = turned(column, columns - b, columns)
         landed = weight_block(r, x, core)
-        remote(landed, landed, weight_send.at[i], weight_recv.at[i], partner).wait_recv()
+        weight_copies[i].wait_recv()
         copy = remote(landed, landed, relay_send.at[i], relay_recv.at[i], partner)
         copy.start()
         relays.append(copy)
-    last = len(plane)
-    landed = weight_block(member, column, 1 - core)
-    remote(landed, landed, weight_send.at[last], weight_recv.at[last], partner).wait_recv()
+    out_copies[1].wait_recv()
+    landed = out_all.at[heads[2], member, dp]
+    out_copies.append(remote(landed, landed, out_send.at[2], out_recv.at[2], across[1]))
+    out_copies[2].start()
+    weight_copies[last].wait_recv()
     for copy in relays:
         copy.wait_recv()
-    for copy in token_copies:
-        copy.wait_recv()
-
-    depth = tokens.shape[1]
-    rows = token_all[...].reshape(own_rows, depth)
-
-    def project(first, count):
+
+    def project(slots, first, count):
+        rows = token_all[slots[0] : slots[-1] + 1].reshape(len(slots) * block, depth)
         weight = weight_all[first : first + count].reshape(count * HEAD_DIM, depth)
         return dot_nt(rows, weight).astype(bf16)
 
-    sent = project(1, 3)
-    for j in range(3):
-        raw[0, j] = sent[:, j * HEAD_DIM : (j + 1) * HEAD_DIM]
     raw_copies = []
-    for a in range(1, members):
-        copy = remote(
-            raw.at[0],
-            raw.at[members - a],
-            raw_send.at[a - 1],
-            raw_recv.at[a - 1],
-            device(head, turned(member, a, members), column, core),
-        )
-        copy.start()
-        raw_copies.append(copy)
-    for copy in out_copies:
-        copy.wait_recv()
+    for slots in GROUPS:
+        for slot in slots:
+            if slot in (1, 3):
+                for piece in range(2):
+                    token_copies[2 * (slot - 1) + piece].wait_recv()
+        sent = project(slots, 1, 3)
+        for n, slot in enumerate(slots):
+            for j in range(3):
+                raw[0, j, heads[slot]] = sent[
+                    n * block : (n + 1) * block, j * HEAD_DIM : (j + 1) * HEAD_DIM
+                ]
+        for slot in slots:
+            for a in range(1, members):
+                at = (a - 1) * HEADS + slot
+                copy = remote(
+                    raw.at[0, :, heads[slot]],
+                    raw.at[members - a, :, heads[slot]],
+                    raw_send.at[at],
+                    raw_recv.at[at],
+                    device(head, turned(member, a, members), column, core),
+                )
+                copy.start()
+                raw_copies.append(copy)
+        query = project(slots, 0, 1)
+        gate = project(slots, 4, 1)
+        for n, slot in enumerate(slots):
+            query_gate[0, heads[slot]] = query[n * block : (n + 1) * block]
+            query_gate[1, heads[slot]] = gate[n * block : (n + 1) * block]
+
+    out_copies[0].wait_recv()
+    out_copies[2].wait_recv()
     plane_copies = []
     mine = out_all.at[:, member, dp]
     for i, where in enumerate(beside + [partner]):
@@ -350,24 +384,32 @@
         copy.start()
         plane_copies.append(copy)
 
-    gate = project(4, 1).astype(f32)
-    query = project(0, 1).astype(f32)
+    gate = query_gate[1].reshape(own_rows, HEAD_DIM).astype(f32)
+    query = query_gate[0].reshape(own_rows, HEAD_DIM).astype(f32)
     queries = query * jax.nn.sigmoid(query)
     gate = gate * jax.nn.sigmoid(gate)
-
+    for copy in local[7:]:
+        copy.wait()
+
+    channels = pl.ds(pl.multiple_of(head * HEAD_DIM, HEAD_DIM), HEAD_DIM)
+
+    def keys_of(a, j):
+        slack_value = small[j : j + 1, channels] / seq_len
+        projected = raw[a, j].reshape(own_rows, HEAD_DIM).astype(f32)
+        key = slack_value * jax.nn.sigmoid(-projected)
+        return key, jnp.log1p(-key)
+
+    made = [(keys_of(0, 0), keys_of(0, 1))]
     for copy in raw_copies:
         copy.wait_recv()
-
-    channels = pl.ds(pl.multiple_of(head * HEAD_DIM, HEAD_DIM), HEAD_DIM)
-
-    def keys_of(j, memory):
-        slack_value = memory[:, channels] / seq_len
-        projected = raw[:, j].reshape(seq_len, HEAD_DIM).astype(f32)
-        key = slack_value * jax.nn.sigmoid(-projected)
-        return key, jnp.log1p(-key)
-
-    key_ahead, log_ahead = keys_of(0, memory_forward)
-    key_behind, log_behind = keys_of(1, memory_backward)
+    for a in range(1, members):
+        made.append((keys_of(a, 0), keys_of(a, 1)))
+
+    def joined(way, item):
+        return jnp.concatenate([one[way][item] for one in made], axis=0)
+
+    key_ahead, log_ahead = joined(0, 0), joined(0, 1)
+    key_behind, log_behind = joined(1, 0), joined(1, 1)
     values = raw[:, 2].reshape(seq_len, HEAD_DIM)
     logs = jnp.concatenate([log_ahead, log_behind], axis=1)
     coarse = logs.astype(bf16)
@@ -396,22 +438,21 @@
         )
     readout = readout.astype(bf16).astype(f32)
     square = jnp.mean(readout * readout, axis=-1, keepdims=True)
-    gated = (readout * lax.rsqrt(square + norm_eps) * norm_gain[...] * gate).astype(bf16)
+    gated = (readout * lax.rsqrt(square + norm_eps) * gain[...] * gate).astype(bf16)
     gated_own[...] = gated.reshape(HEADS, block, HEAD_DIM)
 
     gated_copies = []
     for k in range(1, HEADS):
         copy = remote(
-            gated_own.at[turned(head, k, HEADS)],
+            gated_own.at[heads[k]],
             mixed_heads.at[head],
             gated_send.at[k - 1],
             gated_recv.at[k - 1],
-            across[k - 1],
+            across[k],
         )
         copy.start()
         gated_copies.append(copy)
-    own = pltpu.make_async_copy(gated_own.at[head], mixed_heads.at[head], local_sem.at[0])
-    own.start()
+    mixed_heads[head] = gated_own[head]
 
     back_copies = []
     for i, (a, b) in enumerate(plane):
@@ -425,22 +466,17 @@
     plane_copies[last].wait_recv()
     for copy in back_copies:
         copy.wait_recv()
-    own.wait()
     for copy in gated_copies:
         copy.wait_recv()
 
-    total = jnp.zeros((block, depth), f32)
     weight = out_all[...].reshape(depth, HEADS * HEAD_DIM)
-    joined = jnp.concatenate([mixed_heads[h] for h in range(HEADS)], axis=1)
-    mixed[...] = dot_nt(joined, weight).astype(bf16)
-
-    for copy in token_copies + relays + out_copies + plane_copies + back_copies:
+    row = jnp.concatenate([mixed_heads[h] for h in range(HEADS)], axis=1)
+    mixed[...] = dot_nt(row, weight).astype(bf16)
+
+    for copy in token_copies + weight_copies + relays + out_copies + plane_copies + back_copies:
         copy.wait_send()
     for copy in raw_copies + gated_copies:
         copy.wait_send()
-    mine = weight_block(member, column, core)
-    for i in range(last + 1):
-        remote(mine, mine, weight_send.at[i], weight_recv.at[i], partner).wait_send()
 
 
 def whole_layer(
@@ -466,40 +502,44 @@
     beside = members * columns
     bf16 = jnp.bfloat16
     dma = pltpu.SemaphoreType.DMA
+    hbm = pl.BlockSpec(memory_space=pltpu.HBM)
     vmem = pl.BlockSpec(memory_space=pltpu.VMEM)
     flat = pl.pallas_call(
         functools.partial(layer_kernel, members, columns),
         out_shape=jax.ShapeDtypeStruct((block, depth), bf16),
-        in_specs=[vmem] * 10,
+        in_specs=[hbm] * 10,
         out_specs=vmem,
         scratch_shapes=[
+            pltpu.VMEM((2, HEADS * HEAD_DIM), jnp.float32),
+            pltpu.VMEM((1, HEAD_DIM), jnp.float32),
+            pltpu.VMEM((2, HEADS, block, HEAD_DIM), bf16),
             pltpu.VMEM((HEADS, block, depth), bf16),
             pltpu.VMEM((5, members, 2 * columns, width, depth), bf16),
             pltpu.VMEM((HEADS, members, 2 * columns, out_width, HEADS * HEAD_DIM), bf16),
-            pltpu.VMEM((members, 3, own_rows, HEAD_DIM), bf16),
+            pltpu.VMEM((members, 3, HEADS, block, HEAD_DIM), bf16),
             pltpu.VMEM((HEADS, block, HEAD_DIM), bf16),
             pltpu.VMEM((HEADS, block, HEAD_DIM), bf16),
             pltpu.VMEM((seq_len, seq_len), bf16),
+            dma((2 * others,)),
+            dma((2 * others,)),
+            dma((beside,)),
+            dma((beside,)),
+            dma((beside,)),
+            dma((beside,)),
             dma((others,)),
             dma((others,)),
             dma((beside,)),
             dma((beside,)),
             dma((beside,)),
             dma((beside,)),
+            dma((members * HEADS,)),
+            dma((members * HEADS,)),
             dma((others,)),
             dma((others,)),
-            dma((beside,)),
-            dma((beside,)),
-            dma((beside,)),
-            dma((beside,)),
-            dma((members,)),
-            dma((members,)),
-            dma((others,)),
-            dma((others,)),
-            dma((7,)),
+            dma((10,)),
         ],
         compiler_params=pltpu.CompilerParams(
-            collective_id=0, has_side_effects=True, vmem_limit_bytes=48 * 1024 * 1024
+            collective_id=0, has_side_effects=True, vmem_limit_bytes=67_043_328
         ),
     )(
         tokens.reshape(block, depth),

time: 42.6 us -> 33.8 us (0.79)
  local copies, waits for them, and re-layouts: 6.8 us -> 1.57 us
  Pallas kernels: 35.2 us -> 32.1 us
    unnamed x21 -> x1, local copies, waits for them, and re-layouts: 6.8 us -> 1.57 us
    pallas_call x1, Pallas kernels: 35.2 us -> 32.1 us  [whole_layer(): pl.pallas_call(functools.partial(layer_kernel, members, columns), out_sha...]
where the time goes in v2:
time: 33.8 us; the launch traced here: 33.7 us
  Pallas kernels  32.1 us (95%)
  local copies, waits for them, and re-layouts  1.57 us (5%)
    pallas_call x1, Pallas kernels, whole_layer(): pl.pallas_call(functools.partial(layer_kernel, members, columns), out_sha...  32.1 us
    unnamed x1, local copies, waits for them, and re-layouts  1.57 us

profile of v2, /device:TPU:0, one launch (start us, length us, event | category | flops | bytes accessed | tf_op | source)
XLA Modules:
  0.0 33.7 jit_solution(10589757161245181431)
XLA Ops:
  0.0 32.1 %shard_map.100 = bf16[64,1024]{1,0:T(8,128)(2,1)} custom-call(bf16[64,1024]{1,0:T(8,128)(2,1)} %bitcast.12, bf16[16,1024]{1,0:T(8,128)(2,1)} %bitcast.13, bf16[16,1024]{1,0:T(8,128)(2,1)} %bitcast.14, bf16[16,1024]{1,0:T(8,128)(2,1)} %bitcast.15, bf16[16,1024]{1,0:T(8,128)(2,1)} %bitcast.16, bf16[16,1024]{1,0:T(8,128)(2,1)} %bitcast.17, ...), custom_call_target="tpu_custom_call" | custom-call | tf_op jit(solution)/shard_map/pallas_call | solution.py:507
  32.1 1.6 %copy.12 = bf16[1,64,1024]{2,1,0:T(8,128)(2,1)} copy(bf16[1,64,1024]{2,1,0:T(8,128)(2,1)} %bitcast.11) | data formatting | bytes 262144

commit v3 on v2

--- a/solution.py
+++ b/solution.py
@@ -154,7 +154,8 @@
     return mixed_rows.reshape(seq_count, tok_count, model_width)
 
 
-GROUPS = ((0, 1, 2), (3,))
+GROUPS = ((0, 1), (2,), (3,))
+PIECES = 4
 
 
 def dot_nt(left, right):
@@ -207,7 +208,7 @@
 ):
     bf16, f32 = jnp.bfloat16, jnp.float32
     block, depth = tokens.shape
-    half = block // 2
+    height = block // PIECES
     own_rows = HEADS * block
     sp, dp = lax.axis_index("sp"), lax.axis_index("dp")
     head, member = sp // members, lax.rem(sp, members)
@@ -242,7 +243,7 @@
     ]
     partner = device(head, member, column, 1 - core)
 
-    weights = (w_query, w_forward, w_backward, w_input, w_gate)
+    weights = (w_forward, w_backward, w_input, w_query, w_gate)
     local = []
     for j, weight in enumerate(weights):
         local.append(pltpu.make_async_copy(weight, weight_all.at[j, member, dp], local_sem.at[j]))
@@ -257,7 +258,7 @@
         copy.start()
 
     barrier = pltpu.get_barrier_semaphore()
-    greeted = across[1:] + beside + [partner]
+    greeted = across[1:3] + beside + [partner]
     for where in greeted:
         pl.semaphore_signal(barrier, inc=1, device_id=where, device_id_type=pl.DeviceIdType.MESH)
     pl.semaphore_wait(barrier, len(greeted))
@@ -266,11 +267,11 @@
     local[5].wait()
 
     def rows_of(k, piece):
-        return token_all.at[k, piece * half : (piece + 1) * half]
+        return token_all.at[k, piece * height : (piece + 1) * height]
 
     def send_tokens(source, slot, where):
-        for piece in range(2):
-            at = 2 * (slot - 1) + piece
+        for piece in range(PIECES):
+            at = PIECES * (slot - 1) + piece
             copy = remote(
                 rows_of(source, piece),
                 rows_of(slot, piece),
@@ -285,17 +286,20 @@
     for copy in token_copies:
         copy.start()
 
-    def weight_block(r, x, c):
-        return weight_all.at[:, r, x * 2 + c]
-
+    def weight_block(part, r, x, c):
+        return weight_all.at[part, r, x * 2 + c]
+
+    parts = (slice(0, 3), slice(3, 5))
     for copy in local[:5]:
         copy.wait()
-    mine = weight_block(member, column, core)
-    weight_copies = []
-    for i, where in enumerate(beside + [partner]):
-        copy = remote(mine, mine, weight_send.at[i], weight_recv.at[i], where)
-        copy.start()
-        weight_copies.append(copy)
+    weight_copies = {}
+    for p, part in enumerate(parts):
+        mine = weight_block(part, member, column, core)
+        for i, where in enumerate(beside + [partner]):
+            at = 2 * i + p
+            copy = remote(mine, mine, weight_send.at[at], weight_recv.at[at], where)
+            copy.start()
+            weight_copies[i, p] = copy
     local[6].wait()
     out_mine = out_all.at[head, member, dp]
     out_copies = []
@@ -319,39 +323,64 @@
             )
 
     send_tokens(2, 3, across[1])
-    for piece in range(2):
-        token_copies[2 + piece].wait_recv()
-        token_copies[4 + piece].start()
-
-    relays = []
-    for i, (a, b) in enumerate(plane):
-        r = turned(member, members - a, members)
-        x = turned(column, columns - b, columns)
-        landed = weight_block(r, x, core)
-        weight_copies[i].wait_recv()
-        copy = remote(landed, landed, relay_send.at[i], relay_recv.at[i], partner)
+    for piece in range(PIECES):
+        token_copies[PIECES + piece].wait_recv()
+        token_copies[2 * PIECES + piece].start()
+
+    relays = {}
+
+    def relay_weights(p):
+        for i, (a, b) in enumerate(plane):
+            r = turned(member, members - a, members)
+            x = turned(column, columns - b, columns)
+            landed = weight_block(parts[p], r, x, core)
+            weight_copies[i, p].wait_recv()
+            at = 2 * i + p
+            copy = remote(landed, landed, relay_send.at[at], relay_recv.at[at], partner)
+            copy.start()
+            relays[i, p] = copy
+
+    def weights_there(p):
+        weight_copies[last, p].wait_recv()
+        for i in range(last):
+            relays[i, p].wait_recv()
+
+    plane_copies = {}
+    across_member = device(head, 1 - member, column, core)
+    across_column = device(head, member, 1 - column, core)
+
+    def send_out(slot, kind):
+        owner = 1 - member if kind == 2 else member
+        where = (across_member, across_column, across_column, partner)[kind]
+        landed = out_all.at[heads[slot], owner, dp]
+        at = HEADS * kind + slot
+        copy = remote(landed, landed, plane_send.at[at], plane_recv.at[at], where)
         copy.start()
-        relays.append(copy)
-    out_copies[1].wait_recv()
-    landed = out_all.at[heads[2], member, dp]
-    out_copies.append(remote(landed, landed, out_send.at[2], out_recv.at[2], across[1]))
-    out_copies[2].start()
-    weight_copies[last].wait_recv()
-    for copy in relays:
-        copy.wait_recv()
-
+        plane_copies[kind, slot] = copy
+
+    def spread_out(slot):
+        for kind in (0, 1, 3):
+            send_out(slot, kind)
+
+    def pass_out(slot):
+        plane_copies[0, slot].wait_recv()
+        send_out(slot, 2)
+
+    spread_out(0)
+    relay_weights(0)
     def project(slots, first, count):
         rows = token_all[slots[0] : slots[-1] + 1].reshape(len(slots) * block, depth)
         weight = weight_all[first : first + count].reshape(count * HEAD_DIM, depth)
         return dot_nt(rows, weight).astype(bf16)
 
     raw_copies = []
+    weights_there(0)
     for slots in GROUPS:
         for slot in slots:
             if slot in (1, 3):
-                for piece in range(2):
-                    token_copies[2 * (slot - 1) + piece].wait_recv()
-        sent = project(slots, 1, 3)
+                for piece in range(PIECES):
+                    token_copies[PIECES * (slot - 1) + piece].wait_recv()
+        sent = project(slots, 0, 3)
         for n, slot in enumerate(slots):
             for j in range(3):
                 raw[0, j, heads[slot]] = sent[
@@ -369,20 +398,27 @@
                 )
                 copy.start()
                 raw_copies.append(copy)
-        query = project(slots, 0, 1)
-        gate = project(slots, 4, 1)
-        for n, slot in enumerate(slots):
-            query_gate[0, heads[slot]] = query[n * block : (n + 1) * block]
-            query_gate[1, heads[slot]] = gate[n * block : (n + 1) * block]
-
-    out_copies[0].wait_recv()
+        if slots == GROUPS[0]:
+            relay_weights(1)
+            out_copies[1].wait_recv()
+            landed = out_all.at[heads[2], member, dp]
+            copy = remote(landed, landed, out_send.at[2], out_recv.at[2], across[1])
+            copy.start()
+            out_copies.append(copy)
+            out_copies[0].wait_recv()
+            spread_out(1)
+            spread_out(2)
     out_copies[2].wait_recv()
-    plane_copies = []
-    mine = out_all.at[:, member, dp]
-    for i, where in enumerate(beside + [partner]):
-        copy = remote(mine, mine, plane_send.at[i], plane_recv.at[i], where)
-        copy.start()
-        plane_copies.append(copy)
+    spread_out(3)
+    weights_there(1)
+    sent = project((0, 1, 2, 3), 3, 2)
+    for slot in range(HEADS):
+        for j in range(2):
+            query_gate[j, heads[slot]] = sent[
+                slot * block : (slot + 1) * block, j * HEAD_DIM : (j + 1) * HEAD_DIM
+            ]
+    for slot in range(3):
+        pass_out(slot)
 
     gate = query_gate[1].reshape(own_rows, HEAD_DIM).astype(f32)
     query = query_gate[0].reshape(own_rows, HEAD_DIM).astype(f32)
@@ -400,6 +436,7 @@
         return key, jnp.log1p(-key)
 
     made = [(keys_of(0, 0), keys_of(0, 1))]
+    pass_out(3)
     for copy in raw_copies:
         copy.wait_recv()
     for a in range(1, members):
@@ -455,28 +492,34 @@
     mixed_heads[head] = gated_own[head]
 
     back_copies = []
-    for i, (a, b) in enumerate(plane):
-        r = turned(member, members - a, members)
-        x = turned(column, columns - b, columns)
-        plane_copies[i].wait_recv()
+    for kind, (r, x) in enumerate(
+        ((1 - member, column), (member, 1 - column), (1 - member, 1 - column))
+    ):
+        for slot in range(HEADS):
+            if kind > 0:
+                plane_copies[kind, slot].wait_recv()
         landed = out_all.at[:, r, x * 2 + core]
-        copy = remote(landed, landed, back_send.at[i], back_recv.at[i], partner)
+        copy = remote(landed, landed, back_send.at[kind], back_recv.at[kind], partner)
         copy.start()
         back_copies.append(copy)
-    plane_copies[last].wait_recv()
+    for slot in range(HEADS):
+        plane_copies[3, slot].wait_recv()
     for copy in back_copies:
         copy.wait_recv()
-    for copy in gated_copies:
-        copy.wait_recv()
-
-    weight = out_all[...].reshape(depth, HEADS * HEAD_DIM)
-    row = jnp.concatenate([mixed_heads[h] for h in range(HEADS)], axis=1)
-    mixed[...] = dot_nt(row, weight).astype(bf16)
-
-    for copy in token_copies + weight_copies + relays + out_copies + plane_copies + back_copies:
+    total = jnp.zeros((block, depth), f32)
+    for k in range(HEADS):
+        if k > 0:
+            gated_copies[k - 1].wait_recv()
+        lanes = pl.ds(pl.multiple_of(heads[k] * HEAD_DIM, HEAD_DIM), HEAD_DIM)
+        weight = out_all[:, :, :, :, lanes].reshape(depth, HEAD_DIM)
+        total = total + dot_nt(mixed_heads[heads[k]], weight)
+    mixed[...] = total.astype(bf16)
+
+    for copy in token_copies + out_copies + back_copies + raw_copies + gated_copies:
         copy.wait_send()
-    for copy in raw_copies + gated_copies:
-        copy.wait_send()
+    for copies in (weight_copies, relays, plane_copies):
+        for copy in copies.values():
+            copy.wait_send()
 
 
 def whole_layer(
@@ -520,16 +563,16 @@
             pltpu.VMEM((HEADS, block, HEAD_DIM), bf16),
             pltpu.VMEM((HEADS, block, HEAD_DIM), bf16),
             pltpu.VMEM((seq_len, seq_len), bf16),
-            dma((2 * others,)),
-            dma((2 * others,)),
-            dma((beside,)),
-            dma((beside,)),
-            dma((beside,)),
-            dma((beside,)),
+            dma((PIECES * others,)),
+            dma((PIECES * others,)),
+            dma((2 * beside,)),
+            dma((2 * beside,)),
+            dma((2 * beside,)),
+            dma((2 * beside,)),
             dma((others,)),
             dma((others,)),
-            dma((beside,)),
-            dma((beside,)),
+            dma((HEADS * beside,)),
+            dma((HEADS * beside,)),
             dma((beside,)),
             dma((beside,)),
             dma((members * HEADS,)),
@@ -559,7 +602,8 @@
 def layer(mesh, tokens, w_query, *rest):
     members = mesh.shape["sp"] // HEADS
     columns = mesh.shape["dp"] // 2
-    if tokens.shape[0] == 1 and w_query.shape[1] % 16 == 0:
+    fits = members == 2 and columns == 2 and tokens.shape[0] == 1
+    if fits and w_query.shape[1] % 16 == 0:
         return whole_layer(members, columns, tokens, w_query, *rest)
     return body(tokens, w_query, *rest)
 

time: 33.8 us -> 31.1 us (0.920)
  Pallas kernels: 32.1 us -> 29.4 us
    pallas_call x1, Pallas kernels: 32.1 us -> 29.4 us  [whole_layer(): pl.pallas_call(functools.partial(layer_kernel, members, columns), out_sha...]
where the time goes in v3:
time: 31.1 us; the launch traced here: 30.9 us
  Pallas kernels  29.4 us (95%)
  local copies, waits for them, and re-layouts  1.57 us (5%)
    pallas_call x1, Pallas kernels, whole_layer(): pl.pallas_call(functools.partial(layer_kernel, members, columns), out_sha...  29.4 us
    unnamed x1, local copies, waits for them, and re-layouts  1.57 us

profile of v3, /device:TPU:0, one launch (start us, length us, event | category | flops | bytes accessed | tf_op | source)
XLA Modules:
  0.0 30.9 jit_solution(8176127563996906020)
XLA Ops:
  0.0 29.4 %shard_map.100 = bf16[64,1024]{1,0:T(8,128)(2,1)} custom-call(bf16[64,1024]{1,0:T(8,128)(2,1)} %bitcast.12, bf16[16,1024]{1,0:T(8,128)(2,1)} %bitcast.13, bf16[16,1024]{1,0:T(8,128)(2,1)} %bitcast.14, bf16[16,1024]{1,0:T(8,128)(2,1)} %bitcast.15, bf16[16,1024]{1,0:T(8,128)(2,1)} %bitcast.16, bf16[16,1024]{1,0:T(8,128)(2,1)} %bitcast.17, ...), custom_call_target="tpu_custom_call" | custom-call | tf_op jit(solution)/shard_map/pallas_call | solution.py:550
  29.4 1.6 %copy.12 = bf16[1,64,1024]{2,1,0:T(8,128)(2,1)} copy(bf16[1,64,1024]{2,1,0:T(8,128)(2,1)} %bitcast.11) | data formatting | bytes 262144

commit v4 on v3

--- a/solution.py
+++ b/solution.py
@@ -154,8 +154,8 @@
     return mixed_rows.reshape(seq_count, tok_count, model_width)
 
 
-GROUPS = ((0, 1), (2,), (3,))
-PIECES = 4
+GROUPS = ((0, 1, 2), (3,))
+PIECES = 2
 
 
 def dot_nt(left, right):

time: 31.1 us -> 30.6 us (0.984)
  Pallas kernels: 29.4 us -> 28.9 us
    pallas_call x1, Pallas kernels: 29.4 us -> 28.9 us  [whole_layer(): pl.pallas_call(functools.partial(layer_kernel, members, columns), out_sha...]
where the time goes in v4:
time: 30.6 us; the launch traced here: 30.5 us
  Pallas kernels  28.9 us (94%)
  local copies, waits for them, and re-layouts  1.57 us (5%)
    pallas_call x1, Pallas kernels, whole_layer(): pl.pallas_call(functools.partial(layer_kernel, members, columns), out_sha...  28.9 us
    unnamed x1, local copies, waits for them, and re-layouts  1.57 us

profile of v4, /device:TPU:0, one launch (start us, length us, event | category | flops | bytes accessed | tf_op | source)
XLA Modules:
  0.0 30.5 jit_solution(6964089303918407863)
XLA Ops:
  0.0 28.9 %shard_map.100 = bf16[64,1024]{1,0:T(8,128)(2,1)} custom-call(bf16[64,1024]{1,0:T(8,128)(2,1)} %bitcast.12, bf16[16,1024]{1,0:T(8,128)(2,1)} %bitcast.13, bf16[16,1024]{1,0:T(8,128)(2,1)} %bitcast.14, bf16[16,1024]{1,0:T(8,128)(2,1)} %bitcast.15, bf16[16,1024]{1,0:T(8,128)(2,1)} %bitcast.16, bf16[16,1024]{1,0:T(8,128)(2,1)} %bitcast.17, ...), custom_call_target="tpu_custom_call" | custom-call | tf_op jit(solution)/shard_map/pallas_call | solution.py:550
  28.9 1.6 %copy.12 = bf16[1,64,1024]{2,1,0:T(8,128)(2,1)} copy(bf16[1,64,1024]{2,1,0:T(8,128)(2,1)} %bitcast.11) | data formatting | bytes 262144
